TPU v7x, 128 devices: a whole 4x4x4 slice. The times are simulated.
128 devices in a mesh: sp: 16 (over z, y), dp: 8 (over x, core).
Axes of the slice: x: 4, y: 4, z: 4, core: 2. Of those that a mesh axis runs over, the one named last changes fastest.
Arguments:
- inputs: bfloat16 [8, 3072, 2048], P('dp', 'sp'), may hold values from -6 to 6
- in_gain: float32 [2048], replicated, may hold values from 0.1 to 1.9
- w_query: bfloat16 [2048, 1024], P('dp', 'sp'), may hold values from -0.125 to 0.125
- w_key: bfloat16 [2048, 256], P('dp', 'sp'), may hold values from -0.375 to 0.375
- w_value: bfloat16 [2048, 256], P('dp', 'sp'), may hold values from -0.125 to 0.125
- key_bias: float32 [8, 3072, 16], P('dp', None, 'sp'), may hold values from -20 to 0
- out_gain: float32 [1024], replicated, may hold values from 0.1 to 1.9
- w_out: bfloat16 [1024, 2048], P('sp', 'dp'), may hold values from -0.1875 to 0.1875
Outputs:
- mixed: bfloat16 [8, 3072, 2048], P('dp', 'sp')
All inputs are finite; a program needn't handle non-finite values.
Results may differ from a plain program's by a relative error of at most 0.012.
The roundings to bfloat16 on the way count: a program that leaves them out, or rounds other values in their place, can miss the bound.
Values may be sent and summed in bfloat16 or wider, within the bound.
A program may use at most 128 MiB of HBM per device.

v0:
```python
import jax
import jax.numpy as jnp
from jax import lax
from jax.sharding import PartitionSpec as P

HEAD_DIM = 64
norm_eps = 1e-06


def rows_first(arrays, axis, dims):
    turned = [jnp.moveaxis(a, dim, 0) for a, dim in zip(arrays, dims)]
    both = jnp.concatenate([t.reshape(len(t), -1) for t in turned], axis=1)
    whole, at, finished = (lax.all_gather(both, axis, axis=0, tiled=True), 0, [])
    for t, dim in zip(turned, dims):
        slab = whole[:, at : at + t[0].size].reshape(-1, *t.shape[1:])
        finished.append(jnp.moveaxis(slab, 0, dim))
        at += t[0].size
    return tuple(finished)


def sent_together(arrays, axis, split_dim, concat_dim, along):
    ends, at = ([], 0)
    for a in arrays[:-1]:
        at += a.shape[along]
        ends.append(at)
    both = jnp.concatenate(arrays, axis=along)
    return tuple(
        jnp.split(
            lax.all_to_all(both, axis, split_axis=split_dim, concat_axis=concat_dim, tiled=True),
            ends,
            axis=along,
        )
    )


def body(inputs, in_gain, w_query, w_key, w_value, key_bias, out_gain, w_out):
    width_sp = lax.axis_size("sp")
    own_index = lax.axis_index("sp")
    wide = inputs[0].astype(jnp.float32)
    normed_rows = (
        wide * lax.rsqrt(jnp.mean(wide * wide, axis=-1, keepdims=True) + norm_eps) * in_gain
    ).astype(jnp.bfloat16)
    local_rows = normed_rows.shape[0]
    w_query, w_key, w_value, w_out = rows_first(
        (w_query, w_key, w_value, w_out), "dp", (0, 0, 0, 1)
    )
    w_key, w_value = rows_first((w_key, w_value), "sp", (1, 1))
    keys = jnp.dot(normed_rows, w_key, preferred_element_type=jnp.float32).astype(jnp.bfloat16)
    values = jnp.dot(normed_rows, w_value, preferred_element_type=jnp.float32).astype(jnp.bfloat16)
    queries = jnp.dot(
        normed_rows,
        lax.all_gather(w_query, "sp", axis=1, tiled=True),
        preferred_element_type=jnp.float32,
    ).astype(jnp.bfloat16)
    heads_here = key_bias.shape[2]
    kv_heads = keys.shape[1] // HEAD_DIM
    spread = width_sp // kv_heads
    query_slots = queries.reshape(local_rows, width_sp, heads_here * HEAD_DIM)
    key_copies = jnp.repeat(keys.reshape(local_rows, kv_heads, HEAD_DIM), spread, axis=1)
    value_copies = jnp.repeat(values.reshape(local_rows, kv_heads, HEAD_DIM), spread, axis=1)
    query_all, key_all, value_all = sent_together(
        (query_slots, key_copies, value_copies), "sp", 1, 0, 2
    )
    keys_head = key_all[:, 0, :]
    values_head = value_all[:, 0, :]
    length_all = query_all.shape[0]
    bias_here = key_bias[0].T
    block = min(512, length_all)
    pieces = []
    for index in range(length_all // block):
        start = index * block
        end = start + block
        logits = jnp.einsum(
            "thd,sd->hts", query_all[start:end], keys_head[:end], preferred_element_type=jnp.float32
        )
        logits = logits * HEAD_DIM ** (-0.5) + bias_here[:, None, :end]
        rows = start + jnp.arange(block, dtype=jnp.int32)[:, None]
        columns = jnp.arange(end, dtype=jnp.int32)[None, :]
        strict = (columns < rows)[None, :, :]
        log_keep = jnp.where(strict, jax.nn.log_sigmoid(-logits), jnp.float32(0.0))
        log_rest = lax.cumsum(log_keep, axis=2, reverse=True) - log_keep
        sticks = jnp.where(
            strict, jnp.exp(jax.nn.log_sigmoid(logits) + log_rest), jnp.float32(0.0)
        ).astype(jnp.bfloat16)
        pieces.append(
            jnp.einsum("hts,sd->thd", sticks, values_head[:end], preferred_element_type=jnp.float32)
        )
    attended = jnp.concatenate(pieces, axis=0)
    gains = lax.dynamic_slice_in_dim(
        out_gain, own_index * heads_here * HEAD_DIM, heads_here * HEAD_DIM, 0
    )
    scaled = attended * lax.rsqrt(jnp.mean(attended * attended, axis=-1, keepdims=True) + norm_eps)
    head_out = (scaled * gains.reshape(heads_here, HEAD_DIM)).astype(jnp.bfloat16)
    returned = lax.all_to_all(head_out, "sp", split_axis=0, concat_axis=1, tiled=True)
    returned = returned.reshape(local_rows, width_sp * heads_here * HEAD_DIM)
    mixed = jnp.dot(
        returned,
        lax.all_gather(w_out, "sp", axis=0, tiled=True),
        preferred_element_type=jnp.float32,
    )
    return mixed.astype(jnp.bfloat16)[None]


def solution(mesh):
    placed = (
        P("dp", "sp", None),
        P(),
        P("dp", "sp"),
        P("dp", "sp"),
        P("dp", "sp"),
        P("dp", None, "sp"),
        P(),
        P("sp", "dp"),
    )
    return jax.shard_map(
        body, mesh=mesh, in_specs=placed, out_specs=P("dp", "sp", None), check_vma=False
    )
```

profile of v0, /device:TPU:0, one launch (start us, length us, event | category | flops | bytes accessed | tf_op | source)
XLA Modules:
  0.0 349.7 jit_solution(17781443614021492482)
XLA Ops:
  6.5 0.9 pad_maximum_fusion.2
  7.4 13.7 %all_gather.12 = bf16[2048,160]{0,1:T(8,128)(2,1)S(1)} all-gather(bf16[256,160]{0,1:T(8,128)(2,1)S(1)} %pad_maximum_fusion.2), channel_id=1, replica_groups=mesh['sp'=16,'dp'=8] {'dp'}, dimensions={0}, use_global_device_ids=true | all-gather | bytes 737280 | tf_op jit(solution)/shard_map/all_gather | solution.py:13
  21.1 0.7 pad_maximum_fusion.1
  21.9 0.8 slice_bitcast_fusion.8
  22.7 0.2 fusion.76
  23.0 45.8 %all-gather.6.cloned.1.call-done = bf16[256,4096]{1,0:T(8,128)(2,1)} async-done(((bf16[16,4096]{1,0:T(8,128)(2,1)}), bf16[256,4096]{1,0:T(8,128)(2,1)}) %all-gather.6.cloned.1.call-update) | async-done | bytes 2097168 | tf_op jit(solution)/shard_map/all_gather | solution.py:13
  68.8 1.9 convolution_convert_fusion.2
  70.7 0.1 copy.58
  70.8 0.5 convolution_convert_fusion.3
  71.4 50.3 %all-gather.4.cloned.1.call-done = bf16[2048,1024]{0,1:T(8,128)(2,1)} async-done(((bf16[2048,64]{0,1:T(8,128)(2,1)}), bf16[2048,1024]{0,1:T(8,128)(2,1)}) %all-gather.4.cloned.1.call-update) | async-done | bytes 4194320 | tf_op jit(solution)/shard_map/all_gather | solution.py:52
  121.7 3.7 %convolution_convert_fusion.1 = bf16[192,1024]{1,0:T(8,128)(2,1)S(1)} fusion(bf16[2048,1024]{0,1:T(8,128)(2,1)} %all-gather.4.cloned.1.call-done, bf16[1,192,2048]{2,1,0:T(8,128)(2,1)S(1)} %copy-done.4, f32[2048]{0:T(1024)S(1)} %copy-done.7, f32[192]{0:T(256)S(1)} %add_rsqrt_fusion.1), kind=kOutput, calls=%fused_computation.128 | convolution fusion | flops 807075840 | bytes 5382912 | tf_op jit(solution)/shard_map/dot_general | solution.py:50
  125.5 0.2 copy.56
  125.8 1.4 pad_maximum_fusion
  127.2 5.3 %all-to-all-start = ((bf16[192,16,192]{0,2,1:T(8,128)(2,1)}), bf16[192,16,192]{0,2,1:T(8,128)(2,1)S(1)}, u32[]{:S(2)}, u32[]{:S(2)}) async-start(bf16[192,16,192]{0,2,1:T(8,128)(2,1)} %pad_maximum_fusion), calls=%async_computation | async-start | bytes 3145728 | tf_op jit(solution)/shard_map/all_to_all | solution.py:29
  132.5 0.6 all-gather.8.cloned.1.call-start
  133.1 0.2 all-gather.8.cloned.1.call-update
  133.3 0.8 dynamic_slice.3
  134.2 23.7 %all-to-all-done = bf16[192,16,192]{0,2,1:T(8,128)(2,1)S(1)} async-done(((bf16[192,16,192]{0,2,1:T(8,128)(2,1)}), bf16[192,16,192]{0,2,1:T(8,128)(2,1)S(1)}, u32[]{:S(2)}, u32[]{:S(2)}) %all-to-all-start) | async-done | bytes 1179680 | tf_op jit(solution)/shard_map/all_to_all | solution.py:29
  157.9 0.9 copy.59
  158.7 1.7 all_to_all.27
  160.5 1.6 fusion.116
  162.1 4.8 %fusion.121 = f32[1,512,4,128]{1,2,3,0:T(4,128)S(1)} fusion(f32[1,512,4,128]{1,3,2,0:T(8,128)S(1)} %bitcast.409), kind=kOutput, calls=%fused_computation.155 | output fusion | flops 33292288 | bytes 2097152 | tf_op jit(solution)/shard_map/reduce-window
  166.9 1.3 copy.61
  168.2 2.9 fusion.66
  171.0 5.2 %fusion.74 = f32[1,512,8,128]{1,2,3,0:T(8,128)S(1)} fusion(f32[1,512,8,128]{1,3,2,0:T(8,128)S(1)} %bitcast.404), kind=kOutput, calls=%fused_computation.113 | output fusion | flops 66584576 | bytes 4194304 | tf_op jit(solution)/shard_map/reduce-window.2
  176.2 2.6 copy.63
  178.8 4.1 %fusion.53 = (f32[1,512,1536]{1,2,0:T(8,128)S(1)}, f32[1,512,1536]{1,2,0:T(8,128)}) fusion(s32[512]{0:T(512)S(1)} %iota_add_fusion.3, f32[1536]{0:T(1024)S(1)} %slice_reduce_fusion.1, bf16[3072,1,192]{0,2,1:T(8,128)(2,1)S(1)} %all_to_all.27), kind=kOutput, calls=%fused_computation.82 | convolution fusion | flops 109314048 | bytes 6563840 | tf_op jit(solution)/shard_map/thd,sd->hts/dot_general | solution.py:73
  182.9 10.1 %fusion.42 = f32[1,512,12,128]{1,2,3,0:T(8,128)S(1)} fusion(f32[1,512,12,128]{1,3,2,0:T(8,128)S(1)} %bitcast.402), kind=kOutput, calls=%fused_computation.69 | output fusion | flops 99876864 | bytes 6291456 | tf_op jit(solution)/shard_map/reduce-window.4
  193.0 1.8 copy.65
  194.9 6.1 %fusion.34 = (f32[1,512,2048]{1,2,0:T(8,128)S(1)}, f32[2048,512]{1,0:T(8,128)}) fusion(f32[2048]{0:T(1024)S(1)} %bitcast.419, s32[512]{0:T(512)S(1)} %iota_add_fusion.2, bf16[3072,1,192]{0,2,1:T(8,128)(2,1)} %copy-done.1), kind=kOutput, calls=%fused_computation.56 | convolution fusion | flops 145752064 | bytes 8726528 | tf_op jit(solution)/shard_map/thd,sd->hts/dot_general | solution.py:73
  201.0 10.3 %fusion.40 = f32[1,512,16,128]{1,2,3,0:T(8,128)S(1)} fusion(f32[1,512,16,128]{1,3,2,0:T(8,128)S(1)} %bitcast.401), kind=kOutput, calls=%fused_computation.67 | output fusion | flops 133169152 | bytes 8388608 | tf_op jit(solution)/shard_map/reduce-window.6
  211.3 4.4 %copy.67 = f32[1,512,16,128]{1,3,2,0:T(8,128)} copy(f32[1,512,16,128]{1,2,3,0:T(8,128)S(1)} %fusion.40) | data formatting | bytes 8388608 | tf_op jit(solution)/shard_map/reduce-window.6
  215.7 0.1 reduce-window.51
  215.8 7.1 %fusion.22 = (f32[1,512,2560]{1,2,0:T(8,128)S(1)}, f32[2560,512,1]{1,0,2:T(8,128)}) fusion(s32[512]{0:T(512)S(1)} %iota_add_fusion.1, f32[2560]{0:T(1024)S(1)} %slice_reduce_fusion, bf16[3072,1,192]{0,2,1:T(8,128)(2,1)} %copy-done.1), kind=kOutput, calls=%fused_computation.38 | convolution fusion | flops 182190080 | bytes 10891264 | tf_op jit(solution)/shard_map/thd,sd->hts/dot_general | solution.py:73
  222.9 15.6 %fusion.14 = f32[1,512,20,128]{1,2,3,0:T(8,128)S(1)} fusion(f32[1,512,20,128]{1,3,2,0:T(8,128)S(1)} %bitcast.400), kind=kOutput, calls=%fused_computation.27 | output fusion | flops 166461440 | bytes 10485760 | tf_op jit(solution)/shard_map/reduce-window.8
  238.5 5.4 %copy.69 = f32[1,512,20,128]{1,3,2,0:T(8,128)} copy(f32[1,512,20,128]{1,2,3,0:T(8,128)S(1)} %fusion.14) | data formatting | bytes 10485760 | tf_op jit(solution)/shard_map/reduce-window.8
  243.9 0.1 reduce-window.55
  244.0 8.2 %fusion.6 = (f32[1,512,3072]{1,2,0:T(8,128)S(1)}, f32[3072,512]{1,0:T(8,128)}) fusion(f32[3072]{0:T(1024)S(1)} %bitcast.417, s32[512]{0:T(512)S(1)} %iota_add_fusion, bf16[3072,1,192]{0,2,1:T(8,128)(2,1)} %copy-done.1), kind=kOutput, calls=%fused_computation.14 | convolution fusion | flops 218628096 | bytes 13056000 | tf_op jit(solution)/shard_map/thd,sd->hts/dot_general | solution.py:73
  252.2 15.3 %fusion.12 = f32[1,512,24,128]{1,2,3,0:T(8,128)S(1)} fusion(f32[1,512,24,128]{1,3,2,0:T(8,128)S(1)} %bitcast.398), kind=kOutput, calls=%fused_computation.25 | output fusion | flops 199753728 | bytes 12582912 | tf_op jit(solution)/shard_map/reduce-window.10
  267.5 6.3 %copy.71 = f32[1,512,24,128]{1,3,2,0:T(8,128)} copy(f32[1,512,24,128]{1,2,3,0:T(8,128)S(1)} %fusion.12) | data formatting | bytes 12582912 | tf_op jit(solution)/shard_map/reduce-window.10
  273.8 0.2 reduce-window.59
  274.0 2.6 fusion.114
  276.7 5.8 %fusion.64 = bf16[1,512,1024]{1,2,0:T(8,128)(2,1)S(1)} fusion(f32[1,512,8,128]{1,3,2,0:T(8,128)} %copy.63, f32[1024,512]{1,0:T(8,128)} %get-tuple-element.12, f32[512,8]{0,1:T(8,128)S(1)} %slice_bitcast_fusion.47, f32[1024]{0:T(1024)S(1)} %bitcast.423, s32[512]{0:T(512)S(1)} %iota_add_fusion.4), kind=kLoop, calls=%fused_computation.98 | loop fusion | flops 12582912 | bytes 5265408 | tf_op jit(solution)/shard_map/convert_element_type | solution.py:84
  282.5 6.4 %fusion.51 = bf16[1,512,1536]{1,2,0:T(8,128)(2,1)S(1)} fusion(f32[1,512,12,128]{1,3,2,0:T(8,128)S(1)} %copy.65, f32[1,512,1536]{1,2,0:T(8,128)} %get-tuple-element.14, f32[512,12]{0,1:T(8,128)S(1)} %slice_bitcast_fusion.45, s32[512]{0:T(512)S(1)} %iota_add_fusion.3), kind=kLoop, calls=%fused_computation.80 | loop fusion | flops 17301504 | bytes 7890944 | tf_op jit(solution)/shard_map/convert_element_type | solution.py:84
  288.9 7.3 %fusion.32 = bf16[1,512,2048]{1,2,0:T(8,128)(2,1)S(1)} fusion(f32[1,512,16,128]{1,3,2,0:T(8,128)S(1)} %copy-done, f32[2048,512]{1,0:T(8,128)S(1)} %copy-done.3, f32[512,16]{0,1:T(8,128)S(1)} %slice_bitcast_fusion.43, f32[2048]{0:T(1024)S(1)} %bitcast.420, s32[512]{0:T(512)S(1)} %iota_add_fusion.2), kind=kLoop, calls=%fused_computation.54 | loop fusion | flops 25165824 | bytes 10528768 | tf_op jit(solution)/shard_map/convert_element_type | solution.py:84
  296.3 9.8 %fusion.20 = bf16[1,512,2560]{1,2,0:T(8,128)(2,1)S(1)} fusion(f32[1,512,20,128]{1,3,2,0:T(8,128)S(1)} %bitcast.395, f32[2560,512,1]{1,0,2:T(8,128)} %get-tuple-element.18, f32[512,20]{0,1:T(8,128)S(1)} %slice_bitcast_fusion.41, s32[512]{0:T(512)S(1)} %iota_add_fusion.1), kind=kLoop, calls=%fused_computation.36 | loop fusion | flops 28835840 | bytes 13150208 | tf_op jit(solution)/shard_map/convert_element_type | solution.py:84
  306.2 10.9 %fusion.4 = bf16[1,512,3072]{1,2,0:T(8,128)(2,1)S(1)} fusion(f32[1,512,24,128]{1,3,2,0:T(8,128)S(1)} %bitcast.393, f32[3072,512]{1,0:T(8,128)S(1)} %bitcast.397, f32[512,24]{0,1:T(8,128)S(1)} %slice_bitcast_fusion.39, f32[3072]{0:T(1024)S(1)} %bitcast.418, s32[512]{0:T(512)S(1)} %iota_add_fusion), kind=kLoop, calls=%fused_computation.12 | loop fusion | flops 37748736 | bytes 15792128 | tf_op jit(solution)/shard_map/convert_element_type | solution.py:84
  317.1 0.2 fusion.96
  317.3 0.3 fusion.97
  317.6 0.4 fusion.101
  318.0 0.5 fusion.87
  318.5 0.6 fusion.93
  319.0 0.7 fusion.107
  319.8 0.1 multiply_convert_fusion
  319.9 0.6 broadcast.275
  320.5 0.9 reduce.5
  321.5 0.4 copy.87
  321.8 0.5 reshape.777
  322.4 13.3 %all_to_all.33 = bf16[16,2,6144]{2,1,0:T(2,128)(2,1)S(1)} all-to-all(bf16[16,2,6144]{2,1,0:T(2,128)(2,1)S(1)} %reshape.777), channel_id=1, replica_groups=mesh['sp'=16,'dp'=8] {'sp'}, dimensions={0} | all-to-all | bytes 786432 | tf_op jit(solution)/shard_map/all_to_all | solution.py:94
  335.7 0.8 reshape.778
  336.5 1.5 copy.73
  338.0 0.6 all_to_all.29
  338.6 0.2 copy.74
  338.8 4.1 %fusion.59 = bf16[1,192,2048]{2,1,0:T(8,128)(2,1)} fusion(bf16[192,1024]{0,1:T(8,128)(2,1)S(1)} %bitcast.408, bf16[1024,2048]{1,0:T(8,128)(2,1)} %all-gather.8.cloned.1.call-done), kind=kOutput, calls=%fused_computation.93 | convolution fusion | flops 805699584 | bytes 5373952 | tf_op jit(solution)/shard_map/dot_general | solution.py:96
  (68 shorter events, 0.7 us)
Async XLA Ops:
  6.5 16.2 %copy-start.4 = (bf16[1,192,2048]{2,1,0:T(8,128)(2,1)S(1)}, bf16[1,192,2048]{2,1,0:T(8,128)(2,1)}, u32[]{:S(2)}) copy-start(bf16[1,192,2048]{2,1,0:T(8,128)(2,1)} %param.8) | copy-start | bytes 2359300
  6.5 62.3 %copy-start.7 = (f32[2048]{0:T(1024)S(1)}, f32[2048]{0:T(1024)}, u32[]{:S(2)}) copy-start(f32[2048]{0:T(1024)} %param.9) | copy-start | bytes 24580
  6.5 62.2 %all-gather.6.cloned.1.call-start = ((), (), s32[]{:S(2)}) async-start(), calls=%async_computation.3 | async-start | bytes 2228224 | tf_op jit(solution)/shard_map/all_gather | solution.py:13
  21.8 99.9 %all-gather.4.cloned.1.call-start = ((), (), s32[]{:S(2)}) async-start(), calls=%async_computation.2 | async-start | bytes 4456448 | tf_op jit(solution)/shard_map/all_gather | solution.py:52
  68.8 2.0 copy-start.6
  125.8 7.5 %copy-start.5 = (f32[1,3072,1]{1,2,0:T(1,128)S(1)}, f32[1,3072,1]{1,2,0:T(1,128)}, u32[]{:S(2)}) copy-start(f32[1,3072,1]{1,2,0:T(1,128)} %param.13) | copy-start | bytes 36868
  127.2 30.6 %all-to-all-start = ((bf16[192,16,192]{0,2,1:T(8,128)(2,1)}), bf16[192,16,192]{0,2,1:T(8,128)(2,1)S(1)}, u32[]{:S(2)}, u32[]{:S(2)}) async-start(bf16[192,16,192]{0,2,1:T(8,128)(2,1)} %pad_maximum_fusion), calls=%async_computation | async-start | bytes 3145728 | tf_op jit(solution)/shard_map/all_to_all | solution.py:29
  132.5 206.2 %all-gather.8.cloned.1.call-start = ((), (), s32[]{:S(2)}) async-start(), calls=%async_computation.4 | async-start | bytes 4456448 | tf_op jit(solution)/shard_map/all_gather | solution.py:98
  160.4 18.4 %copy-start.1 = (bf16[3072,1,192]{0,2,1:T(8,128)(2,1)}, bf16[3072,1,192]{0,2,1:T(8,128)(2,1)S(1)}, u32[]{:S(2)}) copy-start(bf16[3072,1,192]{0,2,1:T(8,128)(2,1)S(1)} %all_to_all.27) | copy-start | bytes 3538948
  274.0 14.8 %copy-start.3 = (f32[2048,512]{1,0:T(8,128)S(1)}, f32[2048,512]{1,0:T(8,128)}, u32[]{:S(2)}) copy-start(f32[2048,512]{1,0:T(8,128)} %get-tuple-element.16) | copy-start | bytes 12582916
  276.7 19.6 %slice-start.2 = ((s8[5242880]{0:T(1024)(128)(4,1)}), s8[4194304]{0:T(1024)(128)(4,1)S(1)}, s32[]{:S(2)}) async-start(s8[5242880]{0:T(1024)(128)(4,1)} %bitcast.394), calls=%async_computation.7 | async-start | bytes 8388608
  282.4 6.4 %copy-start = (f32[1,512,16,128]{1,3,2,0:T(8,128)S(1)}, f32[1,512,16,128]{1,3,2,0:T(8,128)}, u32[]{:S(2)}) copy-start(f32[1,512,16,128]{1,3,2,0:T(8,128)} %copy.67) | copy-start | bytes 12582916
  282.4 13.8 %slice-start.3 = ((s8[5242880]{0:T(1024)(128)(4,1)}), s8[1048576]{0:T(1024)(128)(4,1)S(1)}, s32[]{:S(2)}) async-start(s8[5242880]{0:T(1024)(128)(4,1)} %bitcast.394), calls=%async_computation.8 | async-start | bytes 2097152
  288.9 17.3 %slice-start = ((s8[6291456]{0:T(1024)(128)(4,1)}), s8[4194304]{0:T(1024)(128)(4,1)S(1)}, s32[]{:S(2)}) async-start(s8[6291456]{0:T(1024)(128)(4,1)} %bitcast.392), calls=%async_computation.5 | async-start | bytes 8388608
  288.9 17.3 %slice-start.4 = ((s8[6291456]{0:T(1024)(128)(4,1)}), s8[2097152]{0:T(1024)(128)(4,1)S(1)}, s32[]{:S(2)}) async-start(s8[6291456]{0:T(1024)(128)(4,1)} %bitcast.396), calls=%async_computation.9 | async-start | bytes 4194304
  296.2 9.9 %slice-start.1 = ((s8[6291456]{0:T(1024)(128)(4,1)}), s8[2097152]{0:T(1024)(128)(4,1)S(1)}, s32[]{:S(2)}) async-start(s8[6291456]{0:T(1024)(128)(4,1)} %bitcast.392), calls=%async_computation.6 | async-start | bytes 4194304
  296.2 9.9 %slice-start.5 = ((s8[6291456]{0:T(1024)(128)(4,1)}), s8[4194304]{0:T(1024)(128)(4,1)S(1)}, s32[]{:S(2)}) async-start(s8[6291456]{0:T(1024)(128)(4,1)} %bitcast.396), calls=%async_computation.10 | async-start | bytes 8388608
  306.2 10.9 %copy-start.2 = (bf16[3072,1,192]{0,2,1:T(8,128)(2,1)S(1)}, bf16[3072,1,192]{0,2,1:T(8,128)(2,1)}, u32[]{:S(2)}) copy-start(bf16[3072,1,192]{0,2,1:T(8,128)(2,1)} %copy-done.1) | copy-start | bytes 3538948
Sparse Core Ops, SparseCore 0:
  21.9 46.8 all-gather.5
  70.9 50.7 all-gather.3
  135.5 54.9 all-gather.7
where the time goes:
time: 353 us; the launch traced here: 350 us
  waiting for transfers between devices  120 us (34%)
  other arithmetic  109 us (31%)
  matrix products  42.7 us (12%)
  local copies, waits for them, and re-layouts  31.2 us (9%)
  blocking collectives  27 us (8%)
  between operations  14 us (4%)
  starting transfers between devices  5.9 us (2%)
    another operation x12, other arithmetic  61.8 us
    all_gather x1, waiting for transfers between devices, body(): lax.all_gather(w_query, 'sp', axis=1, tiled=True)  50.3 us
    all_gather x1, waiting for transfers between devices, rows_first(): lax.all_gather(both, axis, axis=0, tiled=True)  45.8 us
    convert_element_type x6, other arithmetic, body(): sticks = jnp.where(strict, jnp.exp(jax.nn.log_sigmoid(logits) + log_rest)...  42.8 us
    dot_general x6, matrix products, body(): jnp.einsum('thd,sd->hts', query_all[start:end], keys_head[:end], preferre...  29.9 us
    all_to_all x1, waiting for transfers between devices, sent_together(): lax.all_to_all(both, axis, split_axis=split_dim, concat_axis=concat_dim,...  23.7 us
    another operation x18, local copies, waits for them, and re-layouts  21.8 us
    all_gather x1, blocking collectives, rows_first(): lax.all_gather(both, axis, axis=0, tiled=True)  13.7 us
  transfers between devices with their start and end apart: 4, of which 3 were waited for; matrix products, arithmetic and copies ran while one was open for 48% of the time, Pallas kernels for 0%

commit v1 on v0

--- a/solution.py
+++ b/solution.py
@@ -5,6 +5,11 @@
 
 HEAD_DIM = 64
 norm_eps = 1e-06
+
+
+def gather_by_exchange(value, axis, dim):
+    copies = jnp.concatenate([value] * lax.axis_size(axis), axis=dim)
+    return lax.all_to_all(copies, axis, dim, dim, tiled=True)
 
 
 def rows_first(arrays, axis, dims):
@@ -48,9 +53,7 @@
     keys = jnp.dot(normed_rows, w_key, preferred_element_type=jnp.float32).astype(jnp.bfloat16)
     values = jnp.dot(normed_rows, w_value, preferred_element_type=jnp.float32).astype(jnp.bfloat16)
     queries = jnp.dot(
-        normed_rows,
-        lax.all_gather(w_query, "sp", axis=1, tiled=True),
-        preferred_element_type=jnp.float32,
+        normed_rows, gather_by_exchange(w_query, "sp", 1), preferred_element_type=jnp.float32
     ).astype(jnp.bfloat16)
     heads_here = key_bias.shape[2]
     kv_heads = keys.shape[1] // HEAD_DIM

time: 353 us -> 342 us (0.969)
  waiting for transfers between devices: 120 us -> 99.5 us
  starting transfers between devices: 5.9 us -> 13.4 us
    all_gather x1 -> x0, waiting for transfers between devices: 50.3 us -> none  [body(): lax.all_gather(w_query, 'sp', axis=1, tiled=True)]
    all_gather x1, waiting for transfers between devices: 45.8 us -> 76.7 us  [rows_first(): lax.all_gather(both, axis, axis=0, tiled=True)]
    all_to_all x0 -> x1, starting transfers between devices: none -> 8.23 us  [gather_by_exchange(): return lax.all_to_all(copies, axis, dim, dim, tiled=True)]
  transfers between devices with their start and end apart: 4 -> 4, of which waited for: 3 -> 2; matrix products, arithmetic and copies ran while one was open for 48% -> 50% of each run, Pallas kernels for 0% -> 0%
where the time goes in v1:
time: 342 us; the launch traced here: 338 us
  other arithmetic  108 us (32%)
  waiting for transfers between devices  99.5 us (29%)
  matrix products  43.7 us (13%)
  local copies, waits for them, and re-layouts  33.4 us (10%)
  blocking collectives  25.7 us (8%)
  between operations  14.6 us (4%)
  starting transfers between devices  13.4 us (4%)
    all_gather x1, waiting for transfers between devices, rows_first(): lax.all_gather(both, axis, axis=0, tiled=True)  76.7 us
    another operation x12, other arithmetic  61.9 us
    convert_element_type x6, other arithmetic, body(): sticks = jnp.where(strict, jnp.exp(jax.nn.log_sigmoid(logits) + log_rest)...  41.3 us
    dot_general x6, matrix products, body(): jnp.einsum('thd,sd->hts', query_all[start:end], keys_head[:end], preferre...  29.9 us
    all_to_all x1, waiting for transfers between devices, sent_together(): lax.all_to_all(both, axis, split_axis=split_dim, concat_axis=concat_dim,...  22.2 us
    another operation x18, local copies, waits for them, and re-layouts  21.8 us
    all_gather x1, blocking collectives, rows_first(): lax.all_gather(both, axis, axis=0, tiled=True)  13.7 us
    all_to_all x1, blocking collectives, body(): lax.all_to_all(head_out, 'sp', split_axis=0, concat_axis=1, tiled=True)  12 us
  transfers between devices with their start and end apart: 4, of which 2 were waited for; matrix products, arithmetic and copies ran while one was open for 50% of the time, Pallas kernels for 0%

profile of v1, /device:TPU:0, one launch (start us, length us, event | category | flops | bytes accessed | tf_op | source)
XLA Modules:
  0.0 337.9 jit_solution(15754657176527293575)
XLA Ops:
  6.5 0.8 pad_maximum_fusion.2
  7.4 13.7 %all_gather.9 = bf16[2048,160]{0,1:T(8,128)(2,1)S(1)} all-gather(bf16[256,160]{0,1:T(8,128)(2,1)S(1)} %pad_maximum_fusion.2), channel_id=1, replica_groups=mesh['sp'=16,'dp'=8] {'dp'}, dimensions={0}, use_global_device_ids=true | all-gather | bytes 737280 | tf_op jit(solution)/shard_map/all_gather | solution.py:18
  21.1 0.7 pad_maximum_fusion.1
  21.7 0.7 slice_bitcast_fusion.8
  22.9 2.0 copy-done.3
  24.9 8.2 %all-to-all-start = ((bf16[2048,16,64]{0,2,1:T(8,128)(2,1)}), bf16[2048,16,64]{0,2,1:T(8,128)(2,1)}, u32[]{:S(2)}, u32[]{:S(2)}) async-start(bf16[2048,16,64]{0,2,1:T(8,128)(2,1)} %bitcast.415), calls=%async_computation | async-start | bytes 8388608 | tf_op jit(solution)/shard_map/all_to_all | solution.py:12
  33.1 0.2 fusion.78
  33.4 76.7 %all-gather.3.cloned.1.call-done = bf16[256,4096]{1,0:T(8,128)(2,1)} async-done(((bf16[16,4096]{1,0:T(8,128)(2,1)}), bf16[256,4096]{1,0:T(8,128)(2,1)}) %all-gather.3.cloned.1.call-update) | async-done | bytes 2097168 | tf_op jit(solution)/shard_map/all_gather | solution.py:18
  110.1 1.7 convolution_convert_fusion.2
  111.9 1.7 convolution_convert_fusion.3
  113.8 3.7 %convolution_convert_fusion.1 = bf16[192,1024]{1,0:T(8,128)(2,1)S(1)} fusion(bf16[2048,1024]{0,1:T(8,128)(2,1)} %bitcast.4, bf16[1,192,2048]{2,1,0:T(8,128)(2,1)S(1)} %copy-done.5, f32[2048]{0:T(1024)S(1)} %copy-done.7, f32[192]{0:T(256)S(1)} %add_rsqrt_fusion.1), kind=kOutput, calls=%fused_computation.132 | convolution fusion | flops 807075840 | bytes 5382912 | tf_op jit(solution)/shard_map/dot_general | solution.py:55
  117.6 0.2 copy.56
  117.9 1.4 pad_maximum_fusion
  119.3 4.9 %all-to-all-start.1 = ((bf16[192,16,192]{0,2,1:T(8,128)(2,1)}), bf16[192,16,192]{0,2,1:T(8,128)(2,1)S(1)}, u32[]{:S(2)}, u32[]{:S(2)}) async-start(bf16[192,16,192]{0,2,1:T(8,128)(2,1)} %pad_maximum_fusion), calls=%async_computation.1 | async-start | bytes 3145728 | tf_op jit(solution)/shard_map/all_to_all | solution.py:34
  124.3 0.3 all-gather.5.cloned.1.call-start
  124.5 0.5 all-gather.5.cloned.1.call-update
  125.1 0.8 dynamic_slice.3
  125.9 22.2 %all-to-all-done.1 = bf16[192,16,192]{0,2,1:T(8,128)(2,1)S(1)} async-done(((bf16[192,16,192]{0,2,1:T(8,128)(2,1)}), bf16[192,16,192]{0,2,1:T(8,128)(2,1)S(1)}, u32[]{:S(2)}, u32[]{:S(2)}) %all-to-all-start.1) | async-done | bytes 1179680 | tf_op jit(solution)/shard_map/all_to_all | solution.py:34
  148.2 0.9 copy.59
  149.1 1.7 all_to_all.38
  150.8 1.6 fusion.120
  152.4 4.8 %fusion.125 = f32[1,512,4,128]{1,2,3,0:T(4,128)S(1)} fusion(f32[1,512,4,128]{1,3,2,0:T(8,128)S(1)} %bitcast.424), kind=kOutput, calls=%fused_computation.159 | output fusion | flops 33292288 | bytes 2097152 | tf_op jit(solution)/shard_map/reduce-window
  157.2 1.3 copy.61
  158.5 2.9 fusion.66
  161.3 5.4 %fusion.74 = f32[1,512,8,128]{1,2,3,0:T(8,128)S(1)} fusion(f32[1,512,8,128]{1,3,2,0:T(8,128)S(1)} %bitcast.419), kind=kOutput, calls=%fused_computation.113 | output fusion | flops 66584576 | bytes 4194304 | tf_op jit(solution)/shard_map/reduce-window.2
  166.8 2.6 copy.63
  169.4 4.1 %fusion.53 = (f32[1,512,1536]{1,2,0:T(8,128)S(1)}, f32[1,512,1536]{1,2,0:T(8,128)}) fusion(s32[512]{0:T(512)S(1)} %iota_add_fusion.3, f32[1536]{0:T(1024)S(1)} %slice_reduce_fusion.1, bf16[3072,1,192]{0,2,1:T(8,128)(2,1)S(1)} %all_to_all.38), kind=kOutput, calls=%fused_computation.82 | convolution fusion | flops 109314048 | bytes 6563840 | tf_op jit(solution)/shard_map/thd,sd->hts/dot_general | solution.py:76
  173.4 10.1 %fusion.42 = f32[1,512,12,128]{1,2,3,0:T(8,128)S(1)} fusion(f32[1,512,12,128]{1,3,2,0:T(8,128)S(1)} %bitcast.417), kind=kOutput, calls=%fused_computation.69 | output fusion | flops 99876864 | bytes 6291456 | tf_op jit(solution)/shard_map/reduce-window.4
  183.5 1.8 copy.65
  185.5 6.0 %fusion.34 = (f32[1,512,2048]{1,2,0:T(8,128)S(1)}, f32[2048,512]{1,0:T(8,128)}) fusion(f32[2048]{0:T(1024)S(1)} %bitcast.434, s32[512]{0:T(512)S(1)} %iota_add_fusion.2, bf16[3072,1,192]{0,2,1:T(8,128)(2,1)} %copy-done.1), kind=kOutput, calls=%fused_computation.56 | convolution fusion | flops 145752064 | bytes 8726528 | tf_op jit(solution)/shard_map/thd,sd->hts/dot_general | solution.py:76
  191.5 10.2 %fusion.40 = f32[1,512,16,128]{1,2,3,0:T(8,128)S(1)} fusion(f32[1,512,16,128]{1,3,2,0:T(8,128)S(1)} %bitcast.416), kind=kOutput, calls=%fused_computation.67 | output fusion | flops 133169152 | bytes 8388608 | tf_op jit(solution)/shard_map/reduce-window.6
  201.8 4.4 %copy.67 = f32[1,512,16,128]{1,3,2,0:T(8,128)} copy(f32[1,512,16,128]{1,2,3,0:T(8,128)S(1)} %fusion.40) | data formatting | bytes 8388608 | tf_op jit(solution)/shard_map/reduce-window.6
  206.2 0.1 reduce-window.51
  206.3 7.1 %fusion.22 = (f32[1,512,2560]{1,2,0:T(8,128)S(1)}, f32[2560,512,1]{1,0,2:T(8,128)}) fusion(s32[512]{0:T(512)S(1)} %iota_add_fusion.1, f32[2560]{0:T(1024)S(1)} %slice_reduce_fusion, bf16[3072,1,192]{0,2,1:T(8,128)(2,1)} %copy-done.1), kind=kOutput, calls=%fused_computation.38 | convolution fusion | flops 182190080 | bytes 10891264 | tf_op jit(solution)/shard_map/thd,sd->hts/dot_general | solution.py:76
  213.4 15.5 %fusion.14 = f32[1,512,20,128]{1,2,3,0:T(8,128)S(1)} fusion(f32[1,512,20,128]{1,3,2,0:T(8,128)S(1)} %bitcast.414), kind=kOutput, calls=%fused_computation.27 | output fusion | flops 166461440 | bytes 10485760 | tf_op jit(solution)/shard_map/reduce-window.8
  228.9 5.4 %copy.69 = f32[1,512,20,128]{1,3,2,0:T(8,128)} copy(f32[1,512,20,128]{1,2,3,0:T(8,128)S(1)} %fusion.14) | data formatting | bytes 10485760 | tf_op jit(solution)/shard_map/reduce-window.8
  234.3 0.1 reduce-window.55
  234.5 8.2 %fusion.6 = (f32[1,512,3072]{1,2,0:T(8,128)S(1)}, f32[3072,512]{1,0:T(8,128)}) fusion(f32[3072]{0:T(1024)S(1)} %bitcast.432, s32[512]{0:T(512)S(1)} %iota_add_fusion, bf16[3072,1,192]{0,2,1:T(8,128)(2,1)} %copy-done.1), kind=kOutput, calls=%fused_computation.14 | convolution fusion | flops 218628096 | bytes 13056000 | tf_op jit(solution)/shard_map/thd,sd->hts/dot_general | solution.py:76
  242.6 15.3 %fusion.12 = f32[1,512,24,128]{1,2,3,0:T(8,128)S(1)} fusion(f32[1,512,24,128]{1,3,2,0:T(8,128)S(1)} %bitcast.410), kind=kOutput, calls=%fused_computation.25 | output fusion | flops 199753728 | bytes 12582912 | tf_op jit(solution)/shard_map/reduce-window.10
  257.9 6.3 %copy.71 = f32[1,512,24,128]{1,3,2,0:T(8,128)} copy(f32[1,512,24,128]{1,2,3,0:T(8,128)S(1)} %fusion.12) | data formatting | bytes 12582912 | tf_op jit(solution)/shard_map/reduce-window.10
  264.2 0.2 reduce-window.59
  264.5 2.6 fusion.118
  267.1 5.8 %fusion.64 = bf16[1,512,1024]{1,2,0:T(8,128)(2,1)S(1)} fusion(f32[1,512,8,128]{1,3,2,0:T(8,128)} %copy.63, f32[1024,512]{1,0:T(8,128)} %get-tuple-element.12, f32[512,8]{0,1:T(8,128)S(1)} %slice_bitcast_fusion.47, f32[1024]{0:T(1024)S(1)} %bitcast.438, s32[512]{0:T(512)S(1)} %iota_add_fusion.4), kind=kLoop, calls=%fused_computation.98 | loop fusion | flops 12582912 | bytes 5265408 | tf_op jit(solution)/shard_map/convert_element_type | solution.py:87
  272.9 4.9 %fusion.51 = bf16[1,512,1536]{1,2,0:T(8,128)(2,1)S(1)} fusion(f32[1,512,12,128]{1,3,2,0:T(8,128)S(1)} %copy.65, f32[1,512,1536]{1,2,0:T(8,128)S(1)} %copy-done.4, f32[512,12]{0,1:T(8,128)S(1)} %slice_bitcast_fusion.45, s32[512]{0:T(512)S(1)} %iota_add_fusion.3), kind=kLoop, calls=%fused_computation.80 | loop fusion | flops 17301504 | bytes 7890944 | tf_op jit(solution)/shard_map/convert_element_type | solution.py:87
  277.9 8.9 %fusion.32 = bf16[1,512,2048]{1,2,0:T(8,128)(2,1)S(1)} fusion(f32[1,512,16,128]{1,3,2,0:T(8,128)S(1)} %copy-done, f32[2048,512]{1,0:T(8,128)} %get-tuple-element.16, f32[512,16]{0,1:T(8,128)S(1)} %slice_bitcast_fusion.43, f32[2048]{0:T(1024)S(1)} %bitcast.435, s32[512]{0:T(512)S(1)} %iota_add_fusion.2), kind=kLoop, calls=%fused_computation.54 | loop fusion | flops 25165824 | bytes 10528768 | tf_op jit(solution)/shard_map/convert_element_type | solution.py:87
  286.9 8.2 %fusion.20 = bf16[1,512,2560]{1,2,0:T(8,128)(2,1)S(1)} fusion(f32[1,512,20,128]{1,3,2,0:T(8,128)S(1)} %bitcast.407, f32[2560,512,1]{1,0,2:T(8,128)S(1)} %bitcast.413, f32[512,20]{0,1:T(8,128)S(1)} %slice_bitcast_fusion.41, s32[512]{0:T(512)S(1)} %iota_add_fusion.1), kind=kLoop, calls=%fused_computation.36 | loop fusion | flops 28835840 | bytes 13150208 | tf_op jit(solution)/shard_map/convert_element_type | solution.py:87
  295.2 10.9 %fusion.4 = bf16[1,512,3072]{1,2,0:T(8,128)(2,1)S(1)} fusion(f32[1,512,24,128]{1,3,2,0:T(8,128)S(1)} %bitcast.405, f32[3072,512]{1,0:T(8,128)S(1)} %bitcast.409, f32[512,24]{0,1:T(8,128)S(1)} %slice_bitcast_fusion.39, f32[3072]{0:T(1024)S(1)} %bitcast.433, s32[512]{0:T(512)S(1)} %iota_add_fusion), kind=kLoop, calls=%fused_computation.12 | loop fusion | flops 37748736 | bytes 15792128 | tf_op jit(solution)/shard_map/convert_element_type | solution.py:87
  306.1 0.2 fusion.100
  306.3 0.3 fusion.101
  306.6 0.4 fusion.105
  307.0 0.5 fusion.91
  307.5 0.6 fusion.97
  308.0 0.7 fusion.111
  308.8 0.1 multiply_convert_fusion
  308.9 0.6 broadcast.282
  309.5 0.9 reduce.5
  310.4 0.4 copy.87
  310.8 0.5 reshape.793
  311.4 12.0 %all_to_all.45 = bf16[16,2,6144]{2,1,0:T(2,128)(2,1)S(1)} all-to-all(bf16[16,2,6144]{2,1,0:T(2,128)(2,1)S(1)} %reshape.793), channel_id=1, replica_groups=mesh['sp'=16,'dp'=8] {'sp'}, dimensions={0} | all-to-all | bytes 786432 | tf_op jit(solution)/shard_map/all_to_all | solution.py:97
  323.4 0.8 reshape.794
  324.2 1.5 copy.73
  325.7 0.6 all_to_all.40
  326.3 0.2 copy.74
  326.5 4.1 %fusion.59 = bf16[1,192,2048]{2,1,0:T(8,128)(2,1)} fusion(bf16[192,1024]{0,1:T(8,128)(2,1)S(1)} %bitcast.423, bf16[1024,2048]{1,0:T(8,128)(2,1)} %all-gather.5.cloned.1.call-done), kind=kOutput, calls=%fused_computation.93 | convolution fusion | flops 805699584 | bytes 5373952 | tf_op jit(solution)/shard_map/dot_general | solution.py:99
  (87 shorter events, 1.1 us)
Async XLA Ops:
  6.5 103.5 %all-gather.3.cloned.1.call-start = ((), (), s32[]{:S(2)}) async-start(), calls=%async_computation.3 | async-start | bytes 2228224 | tf_op jit(solution)/shard_map/all_gather | solution.py:18
  22.9 2.0 copy-start.3
  24.9 8.2 %copy-start.5 = (bf16[1,192,2048]{2,1,0:T(8,128)(2,1)S(1)}, bf16[1,192,2048]{2,1,0:T(8,128)(2,1)}, u32[]{:S(2)}) copy-start(bf16[1,192,2048]{2,1,0:T(8,128)(2,1)} %param.8) | copy-start | bytes 2359300
  24.9 85.2 %copy-start.7 = (f32[2048]{0:T(1024)S(1)}, f32[2048]{0:T(1024)}, u32[]{:S(2)}) copy-start(f32[2048]{0:T(1024)} %param.9) | copy-start | bytes 24580
  24.9 88.9 %all-to-all-start = ((bf16[2048,16,64]{0,2,1:T(8,128)(2,1)}), bf16[2048,16,64]{0,2,1:T(8,128)(2,1)}, u32[]{:S(2)}, u32[]{:S(2)}) async-start(bf16[2048,16,64]{0,2,1:T(8,128)(2,1)} %bitcast.415), calls=%async_computation | async-start | bytes 8388608 | tf_op jit(solution)/shard_map/all_to_all | solution.py:12
  117.6 7.5 %copy-start.6 = (f32[1,3072,1]{1,2,0:T(1,128)S(1)}, f32[1,3072,1]{1,2,0:T(1,128)}, u32[]{:S(2)}) copy-start(f32[1,3072,1]{1,2,0:T(1,128)} %param.13) | copy-start | bytes 36868
  119.3 28.9 %all-to-all-start.1 = ((bf16[192,16,192]{0,2,1:T(8,128)(2,1)}), bf16[192,16,192]{0,2,1:T(8,128)(2,1)S(1)}, u32[]{:S(2)}, u32[]{:S(2)}) async-start(bf16[192,16,192]{0,2,1:T(8,128)(2,1)} %pad_maximum_fusion), calls=%async_computation.1 | async-start | bytes 3145728 | tf_op jit(solution)/shard_map/all_to_all | solution.py:34
  124.3 202.2 %all-gather.5.cloned.1.call-start = ((), (), s32[]{:S(2)}) async-start(), calls=%async_computation.4 | async-start | bytes 4456448 | tf_op jit(solution)/shard_map/all_gather | solution.py:101
  150.8 18.6 %copy-start.1 = (bf16[3072,1,192]{0,2,1:T(8,128)(2,1)}, bf16[3072,1,192]{0,2,1:T(8,128)(2,1)S(1)}, u32[]{:S(2)}) copy-start(bf16[3072,1,192]{0,2,1:T(8,128)(2,1)S(1)} %all_to_all.38) | copy-start | bytes 3538948
  264.4 8.5 %copy-start.4 = (f32[1,512,1536]{1,2,0:T(8,128)S(1)}, f32[1,512,1536]{1,2,0:T(8,128)}, u32[]{:S(2)}) copy-start(f32[1,512,1536]{1,2,0:T(8,128)} %get-tuple-element.14) | copy-start | bytes 9437188
  264.5 22.4 %slice-start.6 = ((s8[5242880]{0:T(1024)(128)(4,1)}), s8[4194304]{0:T(1024)(128)(4,1)S(1)}, s32[]{:S(2)}) async-start(s8[5242880]{0:T(1024)(128)(4,1)} %bitcast.412), calls=%async_computation.11 | async-start | bytes 8388608
  267.1 19.8 %slice-start.2 = ((s8[5242880]{0:T(1024)(128)(4,1)}), s8[4194304]{0:T(1024)(128)(4,1)S(1)}, s32[]{:S(2)}) async-start(s8[5242880]{0:T(1024)(128)(4,1)} %bitcast.406), calls=%async_computation.7 | async-start | bytes 8388608
  272.9 5.0 %copy-start = (f32[1,512,16,128]{1,3,2,0:T(8,128)S(1)}, f32[1,512,16,128]{1,3,2,0:T(8,128)}, u32[]{:S(2)}) copy-start(f32[1,512,16,128]{1,3,2,0:T(8,128)} %copy.67) | copy-start | bytes 12582916
  272.9 14.0 %slice-start.3 = ((s8[5242880]{0:T(1024)(128)(4,1)}), s8[1048576]{0:T(1024)(128)(4,1)S(1)}, s32[]{:S(2)}) async-start(s8[5242880]{0:T(1024)(128)(4,1)} %bitcast.406), calls=%async_computation.8 | async-start | bytes 2097152
  272.9 14.0 %slice-start.7 = ((s8[5242880]{0:T(1024)(128)(4,1)}), s8[1048576]{0:T(1024)(128)(4,1)S(1)}, s32[]{:S(2)}) async-start(s8[5242880]{0:T(1024)(128)(4,1)} %bitcast.412), calls=%async_computation.12 | async-start | bytes 2097152
  277.9 17.2 %slice-start = ((s8[6291456]{0:T(1024)(128)(4,1)}), s8[4194304]{0:T(1024)(128)(4,1)S(1)}, s32[]{:S(2)}) async-start(s8[6291456]{0:T(1024)(128)(4,1)} %bitcast.404), calls=%async_computation.5 | async-start | bytes 8388608
  277.9 17.2 %slice-start.4 = ((s8[6291456]{0:T(1024)(128)(4,1)}), s8[2097152]{0:T(1024)(128)(4,1)S(1)}, s32[]{:S(2)}) async-start(s8[6291456]{0:T(1024)(128)(4,1)} %bitcast.408), calls=%async_computation.9 | async-start | bytes 4194304
  286.9 8.2 %slice-start.1 = ((s8[6291456]{0:T(1024)(128)(4,1)}), s8[2097152]{0:T(1024)(128)(4,1)S(1)}, s32[]{:S(2)}) async-start(s8[6291456]{0:T(1024)(128)(4,1)} %bitcast.404), calls=%async_computation.6 | async-start | bytes 4194304
  286.9 8.2 %slice-start.5 = ((s8[6291456]{0:T(1024)(128)(4,1)}), s8[4194304]{0:T(1024)(128)(4,1)S(1)}, s32[]{:S(2)}) async-start(s8[6291456]{0:T(1024)(128)(4,1)} %bitcast.408), calls=%async_computation.10 | async-start | bytes 8388608
  295.2 10.9 %copy-start.2 = (bf16[3072,1,192]{0,2,1:T(8,128)(2,1)S(1)}, bf16[3072,1,192]{0,2,1:T(8,128)(2,1)}, u32[]{:S(2)}) copy-start(bf16[3072,1,192]{0,2,1:T(8,128)(2,1)} %copy-done.1) | copy-start | bytes 3538948
Sparse Core Ops, SparseCore 0:
  21.9 88.1 all-gather.2
  127.2 53.8 all-gather.4
